TPU v7x, 32 devices: a whole 2x2x4 slice. The times are simulated.
32 devices in a mesh: fs: 8 (over z, x), tp: 4 (over y, core).
Axes of the slice: x: 2, y: 2, z: 4, core: 2. Of those that a mesh axis runs over, the one named last changes fastest.
Arguments:
- tokens: bfloat16 [4096, 2048], P('fs', 'tp'), may hold values from -6 to 6
- pre_gain: float32 [2048], replicated, may hold values from 0.1 to 1.9
- pre_gate: float32 [2048, 2816], P('fs', 'tp'), may hold values from -0.125 to 0.125
- pre_up: float32 [2048, 2816], P('fs', 'tp'), may hold values from -0.125 to 0.125
- pre_down: float32 [2816, 2048], P('fs', 'tp'), may hold values from -0.109375 to 0.109375
- mix_gain: float32 [2048], replicated, may hold values from 0.1 to 1.9
- branch_proj: float32 [2048, 1024], P('fs', 'tp'), may hold values from -0.125 to 0.125
- gate_proj: float32 [2048, 1024], P('fs', 'tp'), may hold values from -0.125 to 0.125
- conv_taps: float32 [4, 1024], P(None, 'tp'), may hold values from -3 to 3
- retain_blocks: float32 [16, 64, 64], P('tp'), may hold values from -0.75 to 0.75
- admit_blocks: float32 [16, 64, 64], P('tp'), may hold values from -0.75 to 0.75
- decay_param: float32 [1024], P('tp'), may hold values from 5 to 8.5
- channel_gain: float32 [1024], replicated, may hold values from 0.1 to 1.9
- out_proj: float32 [1024, 2048], P('fs', 'tp'), may hold values from -0.1875 to 0.1875
- post_gain: float32 [2048], replicated, may hold values from 0.1 to 1.9
- post_gate: float32 [2048, 2816], P('fs', 'tp'), may hold values from -0.125 to 0.125
- post_up: float32 [2048, 2816], P('fs', 'tp'), may hold values from -0.125 to 0.125
- post_down: float32 [2816, 2048], P('fs', 'tp'), may hold values from -0.109375 to 0.109375
Outputs:
- layer_out: bfloat16 [4096, 2048], P('fs', 'tp')
All inputs are finite; a program needn't handle non-finite values.
Results may differ from a plain program's by a relative error of at most 0.012.
Values may be sent and summed in bfloat16 or wider, within the bound.
A program may use at most 64 MiB of HBM per device.

v0:
```python
import jax
import jax.numpy as jnp
from jax import lax
from jax.sharding import PartitionSpec as P

SEQ_LEN = 128


EPSILON = 1e-06
DECAY_SCALE = 8.0


def normalize(values, norm_gain):
    floats = values.astype(jnp.float32)
    scaled = floats * lax.rsqrt(jnp.mean(floats * floats, axis=-1, keepdims=True) + EPSILON)
    return (scaled * norm_gain).astype(jnp.bfloat16)


def combine(earlier, latter):
    keep_early, add_early = earlier
    keep_late, add_late = latter
    return (keep_early * keep_late, keep_late * add_early + add_late)


def widen(residual):
    return lax.all_gather(residual, "tp", axis=1, tiled=True)


def contract(operand, stacked):
    return jnp.dot(
        operand,
        lax.all_gather(stacked.astype(jnp.bfloat16), "fs", axis=0, tiled=True),
        preferred_element_type=jnp.float32,
    )


def feed_forward(residual, norm_gain, gate_matrix, up_matrix, down_matrix):
    normed = normalize(widen(residual), norm_gain)
    products = contract(normed, jnp.concatenate((gate_matrix, up_matrix), axis=1))
    split_at = gate_matrix.shape[1]
    hidden = (jax.nn.silu(products[:, :split_at]) * products[:, split_at:]).astype(jnp.bfloat16)
    all_hidden = lax.all_gather(hidden, "tp", axis=1, tiled=True)
    return (residual.astype(jnp.float32) + 0.5 * contract(all_hidden, down_matrix)).astype(
        jnp.bfloat16
    )


def block_gate(convolved, blocks):
    grouped = convolved.reshape(
        convolved.shape[0], convolved.shape[1], blocks.shape[0], blocks.shape[1]
    )
    mixed = jnp.einsum(
        "sthi,hij->sthj", grouped, blocks.astype(jnp.bfloat16), preferred_element_type=jnp.float32
    )
    return jax.nn.sigmoid(mixed).reshape(convolved.shape)


def recurrent_mixer(
    residual,
    norm_gain,
    branch_matrix,
    gate_matrix,
    conv_taps,
    retain_blocks,
    admit_blocks,
    decay_param,
    channel_gain,
    out_matrix,
):
    normed = normalize(widen(residual), norm_gain)
    products = contract(normed, jnp.concatenate((branch_matrix, gate_matrix), axis=1))
    local_width = branch_matrix.shape[1]
    branch = products[:, :local_width]
    gate_act = products[:, local_width:]
    taps_count = conv_taps.shape[0]
    sequences = residual.shape[0] // SEQ_LEN
    framed = branch.reshape(sequences, SEQ_LEN, local_width)
    padded = jnp.pad(framed, ((0, 0), (taps_count - 1, 0), (0, 0)))
    convolved = jnp.zeros_like(framed)
    for tap_index in range(taps_count):
        convolved = convolved + padded[:, tap_index : tap_index + SEQ_LEN] * conv_taps[tap_index]
    convolved = convolved.astype(jnp.bfloat16)
    retained = block_gate(convolved, retain_blocks)
    admitted = block_gate(convolved, admit_blocks)
    log_keep = -DECAY_SCALE * retained * jax.nn.softplus(-decay_param)
    inject = jnp.sqrt(-jnp.expm1(2.0 * log_keep)) * admitted * convolved.astype(jnp.float32)
    _, states = lax.associative_scan(combine, (jnp.exp(log_keep), inject), axis=1)
    mixed_rows = (states.reshape(residual.shape[0], local_width) * jax.nn.gelu(gate_act)).astype(
        jnp.bfloat16
    )
    all_channels = lax.all_gather(mixed_rows, "tp", axis=1, tiled=True)
    mixed_normed = normalize(all_channels, channel_gain)
    return (residual.astype(jnp.float32) + contract(mixed_normed, out_matrix)).astype(jnp.bfloat16)


def local(
    tokens,
    pre_gain,
    pre_gate,
    pre_up,
    pre_down,
    mix_gain,
    branch_proj,
    gate_proj,
    conv_taps,
    retain_blocks,
    admit_blocks,
    decay_param,
    channel_gain,
    out_proj,
    post_gain,
    post_gate,
    post_up,
    post_down,
):
    after_pre = feed_forward(tokens, pre_gain, pre_gate, pre_up, pre_down)
    after_mix = recurrent_mixer(
        after_pre,
        mix_gain,
        branch_proj,
        gate_proj,
        conv_taps,
        retain_blocks,
        admit_blocks,
        decay_param,
        channel_gain,
        out_proj,
    )
    return feed_forward(after_mix, post_gain, post_gate, post_up, post_down)


def solution(mesh):
    placed = (
        P("fs", "tp"),
        P(),
        P("fs", "tp"),
        P("fs", "tp"),
        P("fs", "tp"),
        P(),
        P("fs", "tp"),
        P("fs", "tp"),
        P(None, "tp"),
        P("tp", None, None),
        P("tp", None, None),
        P("tp"),
        P(),
        P("fs", "tp"),
        P(),
        P("fs", "tp"),
        P("fs", "tp"),
        P("fs", "tp"),
    )
    return jax.shard_map(
        local, mesh=mesh, in_specs=placed, out_specs=P("fs", "tp"), check_vma=False
    )
```

profile of v0, /device:TPU:0, one launch (start us, length us, event | category | flops | bytes accessed | tf_op | source)
XLA Modules:
  0.0 807.4 jit_solution(914277624177452306)
XLA Ops:
  10.4 23.8 %all-gather.13.cloned.1.call-done = bf16[512,2048]{1,0:T(8,128)(2,1)} async-done(((bf16[512,512]{1,0:T(8,128)(2,1)}), bf16[512,2048]{1,0:T(8,128)(2,1)}) %all-gather.13.cloned.1.call-update) | async-done | bytes 2097168 | tf_op jit(solution)/shard_map/all_gather | solution.py:26
  36.5 93.0 %all-gather.15.cloned.1.call-done = bf16[2048,1408]{0,1:T(8,128)(2,1)} async-done(((bf16[256,1408]{0,1:T(8,128)(2,1)}), bf16[2048,1408]{0,1:T(8,128)(2,1)}) %all-gather.15.cloned.1.call-update) | async-done | bytes 5767184 | tf_op jit(solution)/shard_map/all_gather | solution.py:32
  129.4 5.8 fusion.16
  137.0 50.1 %all-gather.19.cloned.1.call-done = bf16[2816,512]{1,0:T(8,128)(2,1)} async-done(((bf16[352,512]{1,0:T(8,128)(2,1)}), bf16[2816,512]{1,0:T(8,128)(2,1)}) %all-gather.19.cloned.1.call-update) | async-done | bytes 2883600 | tf_op jit(solution)/shard_map/all_gather | solution.py:32
  187.1 27.1 %all-gather.17.cloned.1.call-done = bf16[512,2816]{0,1:T(8,128)(2,1)} async-done(((bf16[512,704]{0,1:T(8,128)(2,1)}), bf16[512,2816]{0,1:T(8,128)(2,1)}) %all-gather.17.cloned.1.call-update) | async-done | bytes 2883600 | tf_op jit(solution)/shard_map/all_gather | solution.py:42
  214.2 5.2 fusion.29
  220.4 21.7 %all-gather.21.cloned.1.call-done = bf16[512,2048]{1,0:T(8,128)(2,1)} async-done(((bf16[512,512]{1,0:T(8,128)(2,1)}), bf16[512,2048]{1,0:T(8,128)(2,1)}) %all-gather.21.cloned.1.call-update) | async-done | bytes 2097168 | tf_op jit(solution)/shard_map/all_gather | solution.py:26
  244.4 48.9 %all-gather.23.cloned.1.call-done = bf16[2048,512]{1,0:T(8,128)(2,1)} async-done(((bf16[256,512]{1,0:T(8,128)(2,1)}), bf16[2048,512]{1,0:T(8,128)(2,1)}) %all-gather.23.cloned.1.call-update) | async-done | bytes 2097168 | tf_op jit(solution)/shard_map/all_gather | solution.py:32
  299.5 9.4 %slice.212 = f32[4,64,256]{1,2,0:T(8,128)S(1)} slice(f32[4,128,256]{1,2,0:T(8,128)S(1)} %get-tuple-element.6), slice={[0:4:1], [0:127:2], [0:256:1]} | slice | bytes 524288 | tf_op jit(solution)/shard_map/slice | solution.py:87
  308.9 9.1 %slice.213 = f32[4,64,256]{1,2,0:T(8,128)S(1)} slice(f32[4,128,256]{1,2,0:T(8,128)S(1)} %get-tuple-element.6), slice={[0:4:1], [1:128:2], [0:256:1]} | slice | bytes 524288 | tf_op jit(solution)/shard_map/slice | solution.py:87
  317.9 9.1 %slice.211 = f32[4,64,256]{1,2,0:T(8,128)S(1)} slice(f32[4,128,256]{1,2,0:T(8,128)S(1)} %get-tuple-element.5), slice={[0:4:1], [1:128:2], [0:256:1]} | slice | bytes 524288 | tf_op jit(solution)/shard_map/slice | solution.py:87
  327.0 9.5 %slice.215 = f32[4,64,256]{1,2,0:T(8,128)} slice(f32[4,128,256]{1,2,0:T(8,128)S(1)} %get-tuple-element.5), slice={[0:4:1], [0:127:2], [0:256:1]} | slice | bytes 524288 | tf_op jit(solution)/shard_map/slice | solution.py:87
  337.7 4.6 slice.218
  342.3 4.7 slice.219
  347.0 5.3 slice.217
  352.4 5.2 slice.221
  426.4 6.1 slice.216
  432.5 5.2 slice.257
  437.7 9.5 %slice.259 = f32[4,63,256]{1,2,0:T(8,128)} slice(f32[4,128,256]{1,2,0:T(8,128)S(1)} %get-tuple-element.6), slice={[0:4:1], [2:128:2], [0:256:1]} | slice | bytes 516096 | tf_op jit(solution)/shard_map/slice | solution.py:87
  447.2 9.7 %slice.210 = f32[4,63,256]{1,2,0:T(8,128)} slice(f32[4,128,256]{1,2,0:T(8,128)S(1)} %copy-done.1), slice={[0:4:1], [2:128:2], [0:256:1]} | slice | bytes 516096 | tf_op jit(solution)/shard_map/slice | solution.py:87
  502.4 4.5 pad.58
  506.9 4.6 pad.59
  512.4 9.8 %pad.61 = f32[4,128,256]{1,2,0:T(8,128)S(1)} pad(f32[4,64,256]{1,2,0:T(8,128)} %add.195, f32[]{:T(128)} %constant.10.clone.1), padding=0_0_0x1_0_1x0_0_0 | pad | bytes 786436 | tf_op jit(solution)/shard_map/pad | solution.py:87
  522.6 8.8 %pad.60 = f32[4,128,256]{1,2,0:T(8,128)S(1)} pad(f32[4,64,256]{1,2,0:T(8,128)S(1)} %pad_maximum_fusion.4, f32[]{:T(128)} %constant.10.clone.1), padding=0_0_0x0_1_1x0_0_0 | pad | bytes 786436 | tf_op jit(solution)/shard_map/pad | solution.py:87
  533.4 14.7 %all-gather.25.cloned.1.call-done = bf16[512,1024]{1,0:T(8,128)(2,1)} async-done(((bf16[512,256]{1,0:T(8,128)(2,1)}), bf16[512,1024]{1,0:T(8,128)(2,1)}) %all-gather.25.cloned.1.call-update) | async-done | bytes 1048592 | tf_op jit(solution)/shard_map/all_gather | solution.py:91
  549.6 40.9 %all-gather.27.cloned.1.call-done = bf16[1024,512]{1,0:T(8,128)(2,1)} async-done(((bf16[128,512]{1,0:T(8,128)(2,1)}), bf16[1024,512]{1,0:T(8,128)(2,1)}) %all-gather.27.cloned.1.call-update) | async-done | bytes 1048592 | tf_op jit(solution)/shard_map/all_gather | solution.py:32
  596.0 19.1 %all-gather.29.cloned.1.call-done = bf16[512,2048]{1,0:T(8,128)(2,1)} async-done(((bf16[512,512]{1,0:T(8,128)(2,1)}), bf16[512,2048]{1,0:T(8,128)(2,1)}) %all-gather.29.cloned.1.call-update) | async-done | bytes 2097168 | tf_op jit(solution)/shard_map/all_gather | solution.py:26
  617.3 92.8 %all-gather.31.cloned.1.call-done = bf16[2048,1408]{0,1:T(8,128)(2,1)} async-done(((bf16[256,1408]{0,1:T(8,128)(2,1)}), bf16[2048,1408]{0,1:T(8,128)(2,1)}) %all-gather.31.cloned.1.call-update) | async-done | bytes 5767184 | tf_op jit(solution)/shard_map/all_gather | solution.py:32
  710.1 5.8 fusion.12
  717.7 50.2 %all-gather.35.cloned.1.call-done = bf16[2816,512]{1,0:T(8,128)(2,1)} async-done(((bf16[352,512]{1,0:T(8,128)(2,1)}), bf16[2816,512]{1,0:T(8,128)(2,1)}) %all-gather.35.cloned.1.call-update) | async-done | bytes 2883600 | tf_op jit(solution)/shard_map/all_gather | solution.py:32
  767.8 27.1 %all-gather.33.cloned.1.call-done = bf16[512,2816]{0,1:T(8,128)(2,1)} async-done(((bf16[512,704]{0,1:T(8,128)(2,1)}), bf16[512,2816]{0,1:T(8,128)(2,1)}) %all-gather.33.cloned.1.call-update) | async-done | bytes 2883600 | tf_op jit(solution)/shard_map/all_gather | solution.py:42
  794.9 5.2 fusion.28
  (213 shorter events, 146.2 us)
Async XLA Ops:
  6.5 27.7 %all-gather.13.cloned.1.call-start = ((), (), s32[]{:S(2)}) async-start(), calls=%async_computation | async-start | bytes 2621440 | tf_op jit(solution)/shard_map/all_gather | solution.py:26
  7.3 122.1 %all-gather.15.cloned.1.call-start = ((), (), s32[]{:S(2)}) async-start(), calls=%async_computation.1 | async-start | bytes 6488064 | tf_op jit(solution)/shard_map/all_gather | solution.py:32
  9.5 119.9 %copy-start.36 = (f32[2048]{0:T(1024)S(1)}, f32[2048]{0:T(1024)}, u32[]{:S(2)}) copy-start(f32[2048]{0:T(1024)} %param.19) | copy-start | bytes 24580
  9.5 177.6 %all-gather.19.cloned.1.call-start = ((), (), s32[]{:S(2)}) async-start(), calls=%async_computation.3 | async-start | bytes 3244032 | tf_op jit(solution)/shard_map/all_gather | solution.py:32
  10.4 203.8 %all-gather.17.cloned.1.call-start = ((), (), s32[]{:S(2)}) async-start(), calls=%async_computation.2 | async-start | bytes 3604480 | tf_op jit(solution)/shard_map/all_gather | solution.py:42
  34.2 95.2 %copy-start.14 = (bf16[512,2048]{1,0:T(8,128)(2,1)S(1)}, bf16[512,2048]{1,0:T(8,128)(2,1)}, u32[]{:S(2)}) copy-start(bf16[512,2048]{1,0:T(8,128)(2,1)} %all-gather.13.cloned.1.call-done) | copy-start | bytes 6291460
  135.8 78.4 %copy-start.26 = (bf16[512,512]{1,0:T(8,128)(2,1)S(1)}, bf16[512,512]{1,0:T(8,128)(2,1)}, u32[]{:S(2)}) copy-start(bf16[512,512]{1,0:T(8,128)(2,1)} %param.18) | copy-start | bytes 1572868
  136.9 82.5 %copy-start.29 = (f32[256,256]{1,0:T(8,128)S(1)}, f32[256,256]{1,0:T(8,128)}, u32[]{:S(2)}) copy-start(f32[256,256]{1,0:T(8,128)} %param.24) | copy-start | bytes 786436
  137.0 82.5 %copy-start.30 = (f32[256,256]{1,0:T(8,128)S(1)}, f32[256,256]{1,0:T(8,128)}, u32[]{:S(2)}) copy-start(f32[256,256]{1,0:T(8,128)} %param.25) | copy-start | bytes 786436
  137.0 105.2 %all-gather.21.cloned.1.call-start = ((), (), s32[]{:S(2)}) async-start(), calls=%async_computation.4 | async-start | bytes 2621440 | tf_op jit(solution)/shard_map/all_gather | solution.py:26
  219.4 73.8 %copy-start.37 = (f32[2048]{0:T(1024)S(1)}, f32[2048]{0:T(1024)}, u32[]{:S(2)}) copy-start(f32[2048]{0:T(1024)} %param.23) | copy-start | bytes 24580
  219.4 73.8 %all-gather.23.cloned.1.call-start = ((), (), s32[]{:S(2)}) async-start(), calls=%async_computation.5 | async-start | bytes 2359296 | tf_op jit(solution)/shard_map/all_gather | solution.py:32
  220.3 327.8 %all-gather.25.cloned.1.call-start = ((), (), s32[]{:S(2)}) async-start(), calls=%async_computation.6 | async-start | bytes 1310720 | tf_op jit(solution)/shard_map/all_gather | solution.py:91
  242.1 51.1 %copy-start.16 = (bf16[512,2048]{1,0:T(8,128)(2,1)S(1)}, bf16[512,2048]{1,0:T(8,128)(2,1)}, u32[]{:S(2)}) copy-start(bf16[512,2048]{1,0:T(8,128)(2,1)} %all-gather.21.cloned.1.call-done) | copy-start | bytes 6291460
  299.4 27.5 %copy-start = (f32[4,128,256]{1,2,0:T(8,128)}, f32[4,128,256]{1,2,0:T(8,128)S(1)}, u32[]{:S(2)}) copy-start(f32[4,128,256]{1,2,0:T(8,128)S(1)} %get-tuple-element.5) | copy-start | bytes 1572868
  337.7 14.7 %copy-start.2 = (f32[4,64,256]{1,2,0:T(8,128)}, f32[4,64,256]{1,2,0:T(8,128)S(1)}, u32[]{:S(2)}) copy-start(f32[4,64,256]{1,2,0:T(8,128)S(1)} %get-tuple-element.19) | copy-start | bytes 786436
  408.9 11.4 %copy-start.4 = (f32[4,32,256]{1,2,0:T(8,128)S(1)}, f32[4,32,256]{1,2,0:T(8,128)}, u32[]{:S(2)}) copy-start(f32[4,32,256]{1,2,0:T(8,128)} %copy-done.3) | copy-start | bytes 393220
  423.3 23.8 %copy-start.1 = (f32[4,128,256]{1,2,0:T(8,128)S(1)}, f32[4,128,256]{1,2,0:T(8,128)}, u32[]{:S(2)}) copy-start(f32[4,128,256]{1,2,0:T(8,128)} %copy-done) | copy-start | bytes 1572868
  506.9 15.3 %copy-start.10 = (f32[4,63,256]{1,2,0:T(8,128)S(1)}, f32[4,63,256]{1,2,0:T(8,128)}, u32[]{:S(2)}) copy-start(f32[4,63,256]{1,2,0:T(8,128)} %slice.259) | copy-start | bytes 774148
  506.9 15.3 %copy-start.11 = (f32[4,63,256]{1,2,0:T(8,128)S(1)}, f32[4,63,256]{1,2,0:T(8,128)}, u32[]{:S(2)}) copy-start(f32[4,63,256]{1,2,0:T(8,128)} %slice.210) | copy-start | bytes 774148
  531.4 59.1 %copy-start.27 = (bf16[512,512]{1,0:T(8,128)(2,1)S(1)}, bf16[512,512]{1,0:T(8,128)(2,1)}, u32[]{:S(2)}) copy-start(bf16[512,512]{1,0:T(8,128)(2,1)} %fusion.29) | copy-start | bytes 1572868
  531.4 59.1 %copy-start.39 = (f32[1024]{0:T(1024)S(1)}, f32[1024]{0:T(1024)}, u32[]{:S(2)}) copy-start(f32[1024]{0:T(1024)} %param.30) | copy-start | bytes 12292
  532.6 57.9 %all-gather.27.cloned.1.call-start = ((), (), s32[]{:S(2)}) async-start(), calls=%async_computation.7 | async-start | bytes 1179648 | tf_op jit(solution)/shard_map/all_gather | solution.py:32
  533.3 81.7 %all-gather.29.cloned.1.call-start = ((), (), s32[]{:S(2)}) async-start(), calls=%async_computation.8 | async-start | bytes 2621440 | tf_op jit(solution)/shard_map/all_gather | solution.py:26
  549.6 44.4 %copy-start.23 = (f32[256,704]{0,1:T(8,128)S(1)}, f32[256,704]{0,1:T(8,128)}, u32[]{:S(2)}) copy-start(f32[256,704]{0,1:T(8,128)} %param.33) | copy-start | bytes 2162692
  549.6 44.4 %copy-start.24 = (f32[256,704]{0,1:T(8,128)S(1)}, f32[256,704]{0,1:T(8,128)}, u32[]{:S(2)}) copy-start(f32[256,704]{0,1:T(8,128)} %param.34) | copy-start | bytes 2162692
  593.7 116.5 %all-gather.31.cloned.1.call-start = ((), (), s32[]{:S(2)}) async-start(), calls=%async_computation.9 | async-start | bytes 6488064 | tf_op jit(solution)/shard_map/all_gather | solution.py:32
  595.0 115.1 %copy-start.38 = (f32[2048]{0:T(1024)S(1)}, f32[2048]{0:T(1024)}, u32[]{:S(2)}) copy-start(f32[2048]{0:T(1024)} %param.32) | copy-start | bytes 24580
  595.0 172.8 %all-gather.35.cloned.1.call-start = ((), (), s32[]{:S(2)}) async-start(), calls=%async_computation.11 | async-start | bytes 3244032 | tf_op jit(solution)/shard_map/all_gather | solution.py:32
  595.9 199.0 %all-gather.33.cloned.1.call-start = ((), (), s32[]{:S(2)}) async-start(), calls=%async_computation.10 | async-start | bytes 3604480 | tf_op jit(solution)/shard_map/all_gather | solution.py:42
  615.1 95.1 %copy-start.15 = (bf16[512,2048]{1,0:T(8,128)(2,1)S(1)}, bf16[512,2048]{1,0:T(8,128)(2,1)}, u32[]{:S(2)}) copy-start(bf16[512,2048]{1,0:T(8,128)(2,1)} %all-gather.29.cloned.1.call-done) | copy-start | bytes 6291460
  716.5 78.5 %copy-start.28 = (bf16[512,512]{1,0:T(8,128)(2,1)S(1)}, bf16[512,512]{1,0:T(8,128)(2,1)}, u32[]{:S(2)}) copy-start(bf16[512,512]{1,0:T(8,128)(2,1)} %fusion.30) | copy-start | bytes 1572868
  (20 other events, 68.1 us)
Sparse Core Ops, SparseCore 0:
  8.9 25.2 all-gather.12
  36.3 93.1 all-gather.14
  131.6 55.4 all-gather.18
  188.5 25.6 all-gather.16
  219.5 22.5 all-gather.20
  244.1 49.0 all-gather.22
  532.7 15.3 all-gather.24
  550.2 40.2 all-gather.26
  593.8 21.2 all-gather.28
  617.0 93.1 all-gather.30
  712.3 55.4 all-gather.34
  769.3 25.6 all-gather.32
where the time goes:
time: 815 us; the launch traced here: 807 us
  waiting for transfers between devices  510 us (63%)
  local copies, waits for them, and re-layouts  210 us (26%)
  other arithmetic  42.7 us (5%)
  matrix products  28.7 us (4%)
  between operations  14.8 us (2%)
    all_gather x6, waiting for transfers between devices, contract(): lax.all_gather(stacked.astype(jnp.bfloat16), 'fs', axis=0, tiled=True)  376 us
    slice x34, local copies, waits for them, and re-layouts, recurrent_mixer(): lax.associative_scan(combine, (jnp.exp(log_keep), inject), axis=1)  144 us
    all_gather x3, waiting for transfers between devices, widen(): return lax.all_gather(residual, 'tp', axis=1, tiled=True)  64.6 us
    all_gather x2, waiting for transfers between devices, feed_forward(): all_hidden = lax.all_gather(hidden, 'tp', axis=1, tiled=True)  54.2 us
    pad x12, local copies, waits for them, and re-layouts, recurrent_mixer(): lax.associative_scan(combine, (jnp.exp(log_keep), inject), axis=1)  50.5 us
    dot_general x6, matrix products, contract(): jnp.dot(operand, lax.all_gather(stacked.astype(jnp.bfloat16), 'fs', axis=...  28 us
  transfers between devices with their start and end apart: 12, of which 12 were waited for; matrix products, arithmetic and copies ran while one was open for 4% of the time, Pallas kernels for 0%

commit v1 on v0

--- a/solution.py
+++ b/solution.py
@@ -1,6 +1,8 @@
 import jax
 import jax.numpy as jnp
 from jax import lax
+from jax.experimental import pallas as pl
+from jax.experimental.pallas import tpu as pltpu
 from jax.sharding import PartitionSpec as P
 
 SEQ_LEN = 128
@@ -14,12 +16,6 @@
     floats = values.astype(jnp.float32)
     scaled = floats * lax.rsqrt(jnp.mean(floats * floats, axis=-1, keepdims=True) + EPSILON)
     return (scaled * norm_gain).astype(jnp.bfloat16)
-
-
-def combine(earlier, latter):
-    keep_early, add_early = earlier
-    keep_late, add_late = latter
-    return (keep_early * keep_late, keep_late * add_early + add_late)
 
 
 def widen(residual):
@@ -45,14 +41,50 @@
     )
 
 
-def block_gate(convolved, blocks):
-    grouped = convolved.reshape(
-        convolved.shape[0], convolved.shape[1], blocks.shape[0], blocks.shape[1]
+def shifted(values, distance, fill):
+    row = lax.broadcasted_iota(jnp.int32, values.shape, 0)
+    return jnp.where(row >= distance, pltpu.roll(values, distance, 0), fill)
+
+
+def mix_sequence(branch, gate_act, taps, gates, sharpness):
+    width = branch.shape[1]
+    count = taps.shape[0]
+    convolved = branch * taps[count - 1 : count]
+    for back in range(1, count):
+        convolved = convolved + shifted(branch, back, 0.0) * taps[count - 1 - back : count - back]
+    convolved = convolved.astype(jnp.bfloat16)
+    both = jax.nn.sigmoid(jnp.dot(convolved, gates, preferred_element_type=jnp.float32))
+    log_keep = -DECAY_SCALE * both[:, :width] * sharpness
+    keep = jnp.exp(log_keep)
+    inject = (
+        jnp.sqrt(jnp.tanh(-log_keep) * (1.0 + keep * keep))
+        * both[:, width:]
+        * convolved.astype(jnp.float32)
     )
-    mixed = jnp.einsum(
-        "sthi,hij->sthj", grouped, blocks.astype(jnp.bfloat16), preferred_element_type=jnp.float32
+    distance = 1
+    while distance < branch.shape[0]:
+        inject = keep * shifted(inject, distance, 0.0) + inject
+        keep = keep * shifted(keep, distance, 1.0)
+        distance *= 2
+    return (inject * jax.nn.gelu(gate_act)).astype(jnp.bfloat16)
+
+
+def mix_kernel(products_ref, taps_ref, gates_ref, sharp_ref, out_ref):
+    width = out_ref.shape[1]
+    out_ref[...] = mix_sequence(
+        products_ref[:, :width],
+        products_ref[:, width:],
+        taps_ref[...],
+        gates_ref[...],
+        sharp_ref[...],
     )
-    return jax.nn.sigmoid(mixed).reshape(convolved.shape)
+
+
+def spread_blocks(blocks):
+    count, size, _ = blocks.shape
+    eye = jnp.eye(count, dtype=blocks.dtype)
+    wide = eye[:, None, :, None] * blocks[:, :, None, :]
+    return wide.reshape(count * size, count * size).astype(jnp.bfloat16)
 
 
 def recurrent_mixer(
@@ -69,25 +101,26 @@
 ):
     normed = normalize(widen(residual), norm_gain)
     products = contract(normed, jnp.concatenate((branch_matrix, gate_matrix), axis=1))
-    local_width = branch_matrix.shape[1]
-    branch = products[:, :local_width]
-    gate_act = products[:, local_width:]
-    taps_count = conv_taps.shape[0]
-    sequences = residual.shape[0] // SEQ_LEN
-    framed = branch.reshape(sequences, SEQ_LEN, local_width)
-    padded = jnp.pad(framed, ((0, 0), (taps_count - 1, 0), (0, 0)))
-    convolved = jnp.zeros_like(framed)
-    for tap_index in range(taps_count):
-        convolved = convolved + padded[:, tap_index : tap_index + SEQ_LEN] * conv_taps[tap_index]
-    convolved = convolved.astype(jnp.bfloat16)
-    retained = block_gate(convolved, retain_blocks)
-    admitted = block_gate(convolved, admit_blocks)
-    log_keep = -DECAY_SCALE * retained * jax.nn.softplus(-decay_param)
-    inject = jnp.sqrt(-jnp.expm1(2.0 * log_keep)) * admitted * convolved.astype(jnp.float32)
-    _, states = lax.associative_scan(combine, (jnp.exp(log_keep), inject), axis=1)
-    mixed_rows = (states.reshape(residual.shape[0], local_width) * jax.nn.gelu(gate_act)).astype(
-        jnp.bfloat16
-    )
+    width = branch_matrix.shape[1]
+    rows = residual.shape[0]
+    gates = jnp.concatenate((spread_blocks(retain_blocks), spread_blocks(admit_blocks)), axis=1)
+    sharpness = jax.nn.softplus(-decay_param)[None, :]
+    whole = lambda array: pl.BlockSpec(array.shape, lambda i: (0, 0))
+    mixed_rows = pl.pallas_call(
+        mix_kernel,
+        grid=(rows // SEQ_LEN,),
+        in_specs=[
+            pl.BlockSpec((SEQ_LEN, 2 * width), lambda i: (i, 0)),
+            whole(conv_taps),
+            whole(gates),
+            whole(sharpness),
+        ],
+        out_specs=pl.BlockSpec((SEQ_LEN, width), lambda i: (i, 0)),
+        out_shape=jax.ShapeDtypeStruct((rows, width), jnp.bfloat16),
+        cost_estimate=pl.CostEstimate(
+            flops=rows * width * 1200, bytes_accessed=rows * width * 10, transcendentals=0
+        ),
+    )(products, conv_taps, gates, sharpness)
     all_channels = lax.all_gather(mixed_rows, "tp", axis=1, tiled=True)
     mixed_normed = normalize(all_channels, channel_gain)
     return (residual.astype(jnp.float32) + contract(mixed_normed, out_matrix)).astype(jnp.bfloat16)

time: 815 us -> 576 us (0.71)
  local copies, waits for them, and re-layouts: 210 us -> 2.78 us
  other arithmetic: 42.7 us -> 16.9 us
    slice x36 -> x0, local copies, waits for them, and re-layouts: 144 us -> none  [the longest x34 144 us: recurrent_mixer(): lax.associative_scan(combine, (jnp.exp(log_keep), inject), axis=1)]
    pad x12 -> x0, local copies, waits for them, and re-layouts: 50.5 us -> none  [recurrent_mixer(): lax.associative_scan(combine, (jnp.exp(log_keep), inject), axis=1)]
    add x17 -> x0, other arithmetic: 13 us -> none  [the longest x10 6.62 us: combine(): return (keep_early * keep_late, keep_late * add_early + add_late)]
    mul x6 -> x0, other arithmetic: 9.02 us -> none  [the longest x5 9 us: combine(): return (keep_early * keep_late, keep_late * add_early + add_late)]
  transfers between devices with their start and end apart: 12 -> 12, of which waited for: 12 -> 12; matrix products, arithmetic and copies ran while one was open for 4% -> 5% of each run, Pallas kernels for 0% -> 0%
where the time goes in v1:
time: 576 us
  waiting for transfers between devices  508 us (88%)
  matrix products  29 us (5%)
  other arithmetic  16.9 us (3%)
  between operations  13.8 us (2%)
    all_gather x6, waiting for transfers between devices, contract(): lax.all_gather(stacked.astype(jnp.bfloat16), 'fs', axis=0, tiled=True)  376 us
    all_gather x3, waiting for transfers between devices, widen(): return lax.all_gather(residual, 'tp', axis=1, tiled=True)  62.7 us
    all_gather x2, waiting for transfers between devices, feed_forward(): all_hidden = lax.all_gather(hidden, 'tp', axis=1, tiled=True)  54.2 us
    dot_general x6, matrix products, contract(): jnp.dot(operand, lax.all_gather(stacked.astype(jnp.bfloat16), 'fs', axis=...  29 us
    all_gather x1, waiting for transfers between devices, recurrent_mixer(): all_channels = lax.all_gather(mixed_rows, 'tp', axis=1, tiled=True)  14.7 us
  transfers between devices with their start and end apart: 12, of which 12 were waited for; matrix products, arithmetic and copies ran while one was open for 5% of the time, Pallas kernels for 0%

profile of v1, /device:TPU:0, one launch (start us, length us, event | category | flops | bytes accessed | tf_op | source)
XLA Modules:
  0.0 575.8 jit_solution(13669605804205539973)
XLA Ops:
  7.3 1.2 convert.18
  8.6 0.9 pad_maximum_fusion
  9.6 0.8 convert_element_type.86
  10.4 23.8 %all-gather.13.cloned.1.call-done = bf16[512,2048]{1,0:T(8,128)(2,1)} async-done(((bf16[512,512]{1,0:T(8,128)(2,1)}), bf16[512,2048]{1,0:T(8,128)(2,1)}) %all-gather.13.cloned.1.call-update) | async-done | bytes 2097168 | tf_op jit(solution)/shard_map/all_gather | solution.py:22
  34.2 2.2 fusion
  36.5 93.0 %all-gather.15.cloned.1.call-done = bf16[2048,1408]{0,1:T(8,128)(2,1)} async-done(((bf16[256,1408]{0,1:T(8,128)(2,1)}), bf16[2048,1408]{0,1:T(8,128)(2,1)}) %all-gather.15.cloned.1.call-update) | async-done | bytes 5767184 | tf_op jit(solution)/shard_map/all_gather | solution.py:28
  129.4 5.8 %fusion.16 = f32[512,1408]{1,0:T(8,128)S(1)} fusion(bf16[2048,1408]{0,1:T(8,128)(2,1)} %all-gather.15.cloned.1.call-done, bf16[512,2048]{1,0:T(8,128)(2,1)S(1)} %copy-done.1, f32[2048]{0:T(1024)S(1)} %copy-done.17, f32[512]{0:T(512)S(1)} %add_rsqrt_fusion.3), kind=kOutput, calls=%fused_computation.22 | convolution fusion | flops 2956984320 | bytes 10758144 | tf_op jit(solution)/shard_map/dot_general | solution.py:26
  135.8 1.1 copy.19
  137.0 50.1 %all-gather.19.cloned.1.call-done = bf16[2816,512]{1,0:T(8,128)(2,1)} async-done(((bf16[352,512]{1,0:T(8,128)(2,1)}), bf16[2816,512]{1,0:T(8,128)(2,1)}) %all-gather.19.cloned.1.call-update) | async-done | bytes 2883600 | tf_op jit(solution)/shard_map/all_gather | solution.py:28
  187.1 27.1 %all-gather.17.cloned.1.call-done = bf16[512,2816]{0,1:T(8,128)(2,1)} async-done(((bf16[512,704]{0,1:T(8,128)(2,1)}), bf16[512,2816]{0,1:T(8,128)(2,1)}) %all-gather.17.cloned.1.call-update) | async-done | bytes 2883600 | tf_op jit(solution)/shard_map/all_gather | solution.py:38
  214.2 5.2 fusion.29
  219.5 0.7 pad_maximum_fusion.2
  221.1 0.7 pad_maximum_fusion.3.gates_ref
  222.4 19.7 %all-gather.21.cloned.1.call-done = bf16[512,2048]{1,0:T(8,128)(2,1)} async-done(((bf16[512,512]{1,0:T(8,128)(2,1)}), bf16[512,2048]{1,0:T(8,128)(2,1)}) %all-gather.21.cloned.1.call-update) | async-done | bytes 2097168 | tf_op jit(solution)/shard_map/all_gather | solution.py:22
  242.1 2.2 fusion.3
  244.4 48.9 %all-gather.23.cloned.1.call-done = bf16[2048,512]{1,0:T(8,128)(2,1)} async-done(((bf16[256,512]{1,0:T(8,128)(2,1)}), bf16[2048,512]{1,0:T(8,128)(2,1)}) %all-gather.23.cloned.1.call-update) | async-done | bytes 2097168 | tf_op jit(solution)/shard_map/all_gather | solution.py:28
  293.2 3.9 fusion.14.products_ref
  297.1 4.2 shard_map.172
  302.2 14.7 %all-gather.25.cloned.1.call-done = bf16[512,1024]{1,0:T(8,128)(2,1)} async-done(((bf16[512,256]{1,0:T(8,128)(2,1)}), bf16[512,1024]{1,0:T(8,128)(2,1)}) %all-gather.25.cloned.1.call-update) | async-done | bytes 1048592 | tf_op jit(solution)/shard_map/all_gather | solution.py:124
  316.9 1.5 fusion.9
  318.5 40.9 %all-gather.27.cloned.1.call-done = bf16[1024,512]{1,0:T(8,128)(2,1)} async-done(((bf16[128,512]{1,0:T(8,128)(2,1)}), bf16[1024,512]{1,0:T(8,128)(2,1)}) %all-gather.27.cloned.1.call-update) | async-done | bytes 1048592 | tf_op jit(solution)/shard_map/all_gather | solution.py:28
  359.3 3.1 fusion.30
  362.6 0.9 pad_maximum_fusion.1
  363.6 0.8 convert_element_type.104
  364.7 19.2 %all-gather.29.cloned.1.call-done = bf16[512,2048]{1,0:T(8,128)(2,1)} async-done(((bf16[512,512]{1,0:T(8,128)(2,1)}), bf16[512,2048]{1,0:T(8,128)(2,1)}) %all-gather.29.cloned.1.call-update) | async-done | bytes 2097168 | tf_op jit(solution)/shard_map/all_gather | solution.py:22
  383.9 2.2 fusion.6
  386.1 92.8 %all-gather.31.cloned.1.call-done = bf16[2048,1408]{0,1:T(8,128)(2,1)} async-done(((bf16[256,1408]{0,1:T(8,128)(2,1)}), bf16[2048,1408]{0,1:T(8,128)(2,1)}) %all-gather.31.cloned.1.call-update) | async-done | bytes 5767184 | tf_op jit(solution)/shard_map/all_gather | solution.py:28
  479.0 5.8 %fusion.12 = f32[512,1408]{1,0:T(8,128)S(1)} fusion(bf16[2048,1408]{0,1:T(8,128)(2,1)} %all-gather.31.cloned.1.call-done, bf16[512,2048]{1,0:T(8,128)(2,1)S(1)} %copy-done.2, f32[2048]{0:T(1024)S(1)} %copy-done.19, f32[512]{0:T(512)S(1)} %add_rsqrt_fusion), kind=kOutput, calls=%fused_computation.20 | convolution fusion | flops 2956984320 | bytes 10758144 | tf_op jit(solution)/shard_map/dot_general | solution.py:26
  485.3 1.1 copy.20
  486.5 50.2 %all-gather.35.cloned.1.call-done = bf16[2816,512]{1,0:T(8,128)(2,1)} async-done(((bf16[352,512]{1,0:T(8,128)(2,1)}), bf16[2816,512]{1,0:T(8,128)(2,1)}) %all-gather.35.cloned.1.call-update) | async-done | bytes 2883600 | tf_op jit(solution)/shard_map/all_gather | solution.py:28
  536.7 27.1 %all-gather.33.cloned.1.call-done = bf16[512,2816]{0,1:T(8,128)(2,1)} async-done(((bf16[512,704]{0,1:T(8,128)(2,1)}), bf16[512,2816]{0,1:T(8,128)(2,1)}) %all-gather.33.cloned.1.call-update) | async-done | bytes 2883600 | tf_op jit(solution)/shard_map/all_gather | solution.py:38
  563.8 5.2 fusion.28
  (83 shorter events, 4.7 us)
Async XLA Ops:
  6.5 2.0 copy-start.3
  6.5 27.7 %all-gather.13.cloned.1.call-start = ((), (), s32[]{:S(2)}) async-start(), calls=%async_computation | async-start | bytes 2621440 | tf_op jit(solution)/shard_map/all_gather | solution.py:22
  7.3 2.3 copy-start.4
  7.3 122.1 %all-gather.15.cloned.1.call-start = ((), (), s32[]{:S(2)}) async-start(), calls=%async_computation.1 | async-start | bytes 6488064 | tf_op jit(solution)/shard_map/all_gather | solution.py:28
  9.5 119.9 %copy-start.17 = (f32[2048]{0:T(1024)S(1)}, f32[2048]{0:T(1024)}, u32[]{:S(2)}) copy-start(f32[2048]{0:T(1024)} %param.19) | copy-start | bytes 24580
  9.5 177.6 %all-gather.19.cloned.1.call-start = ((), (), s32[]{:S(2)}) async-start(), calls=%async_computation.3 | async-start | bytes 3244032 | tf_op jit(solution)/shard_map/all_gather | solution.py:28
  10.4 203.8 %all-gather.17.cloned.1.call-start = ((), (), s32[]{:S(2)}) async-start(), calls=%async_computation.2 | async-start | bytes 3604480 | tf_op jit(solution)/shard_map/all_gather | solution.py:38
  34.2 95.2 %copy-start.1 = (bf16[512,2048]{1,0:T(8,128)(2,1)S(1)}, bf16[512,2048]{1,0:T(8,128)(2,1)}, u32[]{:S(2)}) copy-start(bf16[512,2048]{1,0:T(8,128)(2,1)} %all-gather.13.cloned.1.call-done) | copy-start | bytes 6291460
  135.8 78.4 %copy-start.8 = (bf16[512,512]{1,0:T(8,128)(2,1)S(1)}, bf16[512,512]{1,0:T(8,128)(2,1)}, u32[]{:S(2)}) copy-start(bf16[512,512]{1,0:T(8,128)(2,1)} %param.18) | copy-start | bytes 1572868
  136.9 82.5 %copy-start.11 = (f32[256,256]{1,0:T(8,128)S(1)}, f32[256,256]{1,0:T(8,128)}, u32[]{:S(2)}) copy-start(f32[256,256]{1,0:T(8,128)} %param.24) | copy-start | bytes 786436
  136.9 82.6 %copy-start.12 = (f32[256,256]{1,0:T(8,128)S(1)}, f32[256,256]{1,0:T(8,128)}, u32[]{:S(2)}) copy-start(f32[256,256]{1,0:T(8,128)} %param.25) | copy-start | bytes 786436
  137.0 105.2 %all-gather.21.cloned.1.call-start = ((), (), s32[]{:S(2)}) async-start(), calls=%async_computation.4 | async-start | bytes 2621440 | tf_op jit(solution)/shard_map/all_gather | solution.py:22
  219.4 1.0 copy-start.15
  219.4 2.4 copy-start.16
  219.4 73.8 %all-gather.23.cloned.1.call-start = ((), (), s32[]{:S(2)}) async-start(), calls=%async_computation.5 | async-start | bytes 2359296 | tf_op jit(solution)/shard_map/all_gather | solution.py:28
  220.3 96.6 %all-gather.25.cloned.1.call-start = ((), (), s32[]{:S(2)}) async-start(), calls=%async_computation.6 | async-start | bytes 1310720 | tf_op jit(solution)/shard_map/all_gather | solution.py:124
  220.4 72.9 %copy-start.18 = (f32[2048]{0:T(1024)S(1)}, f32[2048]{0:T(1024)}, u32[]{:S(2)}) copy-start(f32[2048]{0:T(1024)} %param.23) | copy-start | bytes 24580
  242.1 51.1 %copy-start = (bf16[512,2048]{1,0:T(8,128)(2,1)S(1)}, bf16[512,2048]{1,0:T(8,128)(2,1)}, u32[]{:S(2)}) copy-start(bf16[512,2048]{1,0:T(8,128)(2,1)} %all-gather.21.cloned.1.call-done) | copy-start | bytes 6291460
  244.4 57.1 %copy-start.13 = (f32[128,512]{1,0:T(8,128)S(1)}, f32[128,512]{1,0:T(8,128)}, u32[]{:S(2)}) copy-start(f32[128,512]{1,0:T(8,128)} %param.31) | copy-start | bytes 786436
  297.1 62.2 %copy-start.9 = (bf16[512,512]{1,0:T(8,128)(2,1)S(1)}, bf16[512,512]{1,0:T(8,128)(2,1)}, u32[]{:S(2)}) copy-start(bf16[512,512]{1,0:T(8,128)(2,1)} %fusion.29) | copy-start | bytes 1572868
  297.1 62.2 %copy-start.20 = (f32[1024]{0:T(1024)S(1)}, f32[1024]{0:T(1024)}, u32[]{:S(2)}) copy-start(f32[1024]{0:T(1024)} %param.30) | copy-start | bytes 12292
  301.4 57.9 %all-gather.27.cloned.1.call-start = ((), (), s32[]{:S(2)}) async-start(), calls=%async_computation.7 | async-start | bytes 1179648 | tf_op jit(solution)/shard_map/all_gather | solution.py:28
  302.2 81.7 %all-gather.29.cloned.1.call-start = ((), (), s32[]{:S(2)}) async-start(), calls=%async_computation.8 | async-start | bytes 2621440 | tf_op jit(solution)/shard_map/all_gather | solution.py:22
  318.4 44.1 %copy-start.5 = (f32[256,704]{0,1:T(8,128)S(1)}, f32[256,704]{0,1:T(8,128)}, u32[]{:S(2)}) copy-start(f32[256,704]{0,1:T(8,128)} %param.33) | copy-start | bytes 2162692
  318.4 44.1 %copy-start.6 = (f32[256,704]{0,1:T(8,128)S(1)}, f32[256,704]{0,1:T(8,128)}, u32[]{:S(2)}) copy-start(f32[256,704]{0,1:T(8,128)} %param.34) | copy-start | bytes 2162692
  362.5 1.2 copy-start.7
  362.5 116.5 %all-gather.31.cloned.1.call-start = ((), (), s32[]{:S(2)}) async-start(), calls=%async_computation.9 | async-start | bytes 6488064 | tf_op jit(solution)/shard_map/all_gather | solution.py:28
  363.5 115.4 %copy-start.19 = (f32[2048]{0:T(1024)S(1)}, f32[2048]{0:T(1024)}, u32[]{:S(2)}) copy-start(f32[2048]{0:T(1024)} %param.32) | copy-start | bytes 24580
  363.6 173.1 %all-gather.35.cloned.1.call-start = ((), (), s32[]{:S(2)}) async-start(), calls=%async_computation.11 | async-start | bytes 3244032 | tf_op jit(solution)/shard_map/all_gather | solution.py:28
  364.5 199.3 %all-gather.33.cloned.1.call-start = ((), (), s32[]{:S(2)}) async-start(), calls=%async_computation.10 | async-start | bytes 3604480 | tf_op jit(solution)/shard_map/all_gather | solution.py:38
  383.9 95.1 %copy-start.2 = (bf16[512,2048]{1,0:T(8,128)(2,1)S(1)}, bf16[512,2048]{1,0:T(8,128)(2,1)}, u32[]{:S(2)}) copy-start(bf16[512,2048]{1,0:T(8,128)(2,1)} %all-gather.29.cloned.1.call-done) | copy-start | bytes 6291460
  485.3 78.5 %copy-start.10 = (bf16[512,512]{1,0:T(8,128)(2,1)S(1)}, bf16[512,512]{1,0:T(8,128)(2,1)}, u32[]{:S(2)}) copy-start(bf16[512,512]{1,0:T(8,128)(2,1)} %fusion.30) | copy-start | bytes 1572868
  (1 other events, 1.0 us)
Sparse Core Ops, SparseCore 0:
  8.9 25.2 all-gather.12
  36.3 93.1 all-gather.14
  131.6 55.4 all-gather.18
  188.5 25.6 all-gather.16
  219.5 22.5 all-gather.20
  244.1 49.0 all-gather.22
  301.5 15.3 all-gather.24
  319.0 40.2 all-gather.26
  362.6 21.2 all-gather.28
  385.8 93.1 all-gather.30
  481.1 55.4 all-gather.34
  538.1 25.6 all-gather.32

commit v2 on v1

--- a/solution.py
+++ b/solution.py
@@ -1,3 +1,5 @@
+import functools
+
 import jax
 import jax.numpy as jnp
 from jax import lax
@@ -126,6 +128,389 @@
     return (residual.astype(jnp.float32) + contract(mixed_normed, out_matrix)).astype(jnp.bfloat16)
 
 
+ROW_TILE = 256
+MESH = pl.DeviceIdType.MESH
+
+
+class Exchange:
+    def __init__(self):
+        self.sent = []
+
+    def send(self, source, target, send_sem, recv_sem, device, condition=None):
+        copy = pltpu.make_async_remote_copy(
+            src_ref=source,
+            dst_ref=target,
+            send_sem=send_sem,
+            recv_sem=recv_sem,
+            device_id=device,
+            device_id_type=MESH,
+        )
+        when(condition, copy.start)
+        self.sent.append((copy, condition))
+
+    def drain(self):
+        for copy, condition in self.sent:
+            when(condition, copy.wait_send)
+
+
+def when(condition, action):
+    if condition is None:
+        action()
+    else:
+        pl.when(condition)(action)
+
+
+def layer_kernel(fs_size, tp_size, *refs):
+    (tokens, pre_gain, mix_gain, channel_gain, post_gain, taps, gates, sharpness) = refs[:8]
+    shards = refs[8:16]
+    out = refs[16]
+    whole = refs[17:25]
+    first, second, third, hidden_one, hidden_two, channels, normed = refs[25:32]
+    recv_sem, line_sem, back_sem, pair_sem, keep_sem = refs[32:37]
+    tp_recv, tp_peer, tp_own, tp_pass, token_sem = refs[37:42]
+
+    f = lax.axis_index("fs")
+    t = lax.axis_index("tp")
+    x = lax.rem(f, 2)
+    z = f // 2
+    depth = fs_size // 2
+    half = tp_size // 2
+    across = {"fs": f + 1 - 2 * x}
+    above = {"fs": lax.rem(f + 2, fs_size)}
+    below = {"fs": lax.rem(f + fs_size - 2, fs_size)}
+    has_above = z < depth - 1
+    has_below = z > 0
+    twin = t + 1 - 2 * lax.rem(t, 2)
+    peers = [lax.rem(t + 2 * k, tp_size) for k in range(1, half)]
+    links = Exchange()
+
+    barrier = pltpu.get_barrier_semaphore()
+    greeted = [(across, None), (above, has_above), (below, has_below), ({"tp": twin}, None)]
+    greeted += [({"tp": peer}, None) for peer in peers]
+    for device, condition in greeted:
+        when(
+            condition,
+            functools.partial(
+                pl.semaphore_signal, barrier, inc=1, device_id=device, device_id_type=MESH
+            ),
+        )
+    line_ends = (z == 0).astype(jnp.int32) + (z == depth - 1).astype(jnp.int32)
+    pl.semaphore_wait(barrier, len(greeted) - line_ends)
+
+    def shard_at(p, owner):
+        rows = shards[p].shape[0]
+        return whole[p].at[pl.ds(pl.multiple_of(owner * rows, rows), rows)]
+
+    def arrive(p, owner, condition=None):
+        place = shard_at(p, owner)
+        copy = pltpu.make_async_remote_copy(
+            src_ref=place,
+            dst_ref=place,
+            send_sem=pair_sem.at[p, 0],
+            recv_sem=recv_sem.at[p, owner],
+            device_id=across,
+            device_id_type=MESH,
+        )
+        when(condition, copy.wait_recv)
+
+    def own_copy(p):
+        return pltpu.make_async_copy(shards[p], shard_at(p, f), keep_sem.at[p])
+
+    def launch(p):
+        place, sem = shard_at(p, f), recv_sem.at[p, f]
+        links.send(shards[p], place, line_sem.at[p, f], sem, above, has_above)
+        links.send(shards[p], place, back_sem.at[p, 0], sem, below, has_below)
+        links.send(shards[p], place, pair_sem.at[p, z], sem, across)
+        own_copy(p).start()
+
+    def launch_pair(p):
+        owner = f + 1 - 2 * x
+        arrive(p, owner)
+        place, sem = shard_at(p, owner), recv_sem.at[p, owner]
+        links.send(place, place, line_sem.at[p, owner], sem, above, has_above)
+        links.send(place, place, back_sem.at[p, 1], sem, below, has_below)
+
+    def relay(p, distance, column, cross):
+        for sign, edge, there in ((-1, above, has_above), (1, below, has_below)):
+            level = z + sign * distance
+            exists = (level >= 0) & (level < depth)
+            level = lax.rem(level + depth, depth)
+            owner = level * 2 + column
+            arrive(p, owner, exists)
+            place, sem = shard_at(p, owner), recv_sem.at[p, owner]
+            links.send(place, place, line_sem.at[p, owner], sem, edge, exists & there)
+            if cross:
+                links.send(place, place, pair_sem.at[p, level], sem, across, exists)
+
+    count = len(shards)
+    direct = (2,)
+
+    def step(number):
+        for p in range(count):
+            if max(p - 1, 0) == number:
+                launch(p)
+        for p in range(count):
+            if p in direct:
+                if p + 1 == number:
+                    launch_pair(p)
+                if 1 <= number - p - 1 < depth:
+                    relay(p, number - p - 1, 1 - x, False)
+            if 1 <= number - p < depth:
+                relay(p, number - p, x, p not in direct)
+
+    def ready(p):
+        own_copy(p).wait()
+        if p not in direct:
+            for level in range(depth):
+                arrive(p, level * 2 + 1 - x)
+
+    def spread(array, index):
+        for k, peer in enumerate(peers):
+            links.send(
+                array.at[t], array.at[t], tp_peer.at[index, k], tp_recv.at[index, t], {"tp": peer}
+            )
+        links.send(
+            array.at[t], array.at[t], tp_own.at[index], tp_recv.at[index, t], {"tp": twin}
+        )
+
+    def landed(array, index, slot):
+        pltpu.make_async_remote_copy(
+            src_ref=array.at[slot],
+            dst_ref=array.at[slot],
+            send_sem=tp_own.at[index],
+            recv_sem=tp_recv.at[index, slot],
+            device_id={"tp": twin},
+            device_id_type=MESH,
+        ).wait_recv()
+
+    def collect(array, index):
+        for k, peer in enumerate(peers):
+            landed(array, index, peer)
+            links.send(
+                array.at[peer],
+                array.at[peer],
+                tp_pass.at[index, k],
+                tp_recv.at[index, peer],
+                {"tp": twin},
+            )
+        landed(array, index, twin)
+        for k in range(1, half):
+            landed(array, index, lax.rem(twin + 2 * k, tp_size))
+
+    total_rows = tokens.shape[0]
+
+    def tiles(size, body):
+        def run(i, carry):
+            body(pl.ds(pl.multiple_of(i * size, size), size))
+            return carry
+
+        lax.fori_loop(0, total_rows // size, run, 0)
+
+    def norm_slots(array, gain):
+        width = array.shape[2]
+        features = width * tp_size
+
+        def body(rows):
+            parts = [array[s, rows, :].astype(jnp.float32) for s in range(tp_size)]
+            squares = sum(jnp.sum(part * part, axis=-1, keepdims=True) for part in parts)
+            scale = lax.rsqrt(squares / features + EPSILON)
+            for s, part in enumerate(parts):
+                at = slice(s * width, (s + 1) * width)
+                normed[rows, at] = (part * scale * gain[:, at]).astype(jnp.bfloat16)
+
+        tiles(64, body)
+
+    def dot(left, right):
+        return jnp.dot(left, right, preferred_element_type=jnp.float32)
+
+    def gated(gate, up, hidden):
+        def body(rows):
+            values = normed[rows, :]
+            product = jax.nn.silu(dot(values, gate[...])) * dot(values, up[...])
+            hidden[t, rows, :] = product.astype(jnp.bfloat16)
+
+        tiles(ROW_TILE, body)
+
+    def lower(hidden, down, residual, store):
+        width = hidden.shape[2]
+
+        def body(rows):
+            total = sum(
+                dot(hidden[s, rows, :], down[s * width : (s + 1) * width, :])
+                for s in range(tp_size)
+            )
+            value = residual[t, rows, :].astype(jnp.float32) + 0.5 * total
+            store(rows, value.astype(jnp.bfloat16))
+
+        tiles(ROW_TILE, body)
+
+    def mix(rows):
+        width = channels.shape[2]
+        products = dot(normed[rows, :], whole[3][...])
+        channels[t, rows, :] = mix_sequence(
+            products[:, :width], products[:, width:], taps[...], gates[...], sharpness[...]
+        )
+
+    def put(array):
+        def store(rows, value):
+            array[t, rows, :] = value
+
+        return store
+
+    def finish(rows, value):
+        out[rows, :] = value
+
+    def project(rows):
+        width = channels.shape[2] * tp_size
+        total = dot(normed[rows, :width], whole[4][...])
+        third[t, rows, :] = (second[t, rows, :].astype(jnp.float32) + total).astype(jnp.bfloat16)
+
+    local_tokens = pltpu.make_async_copy(tokens, first.at[t], token_sem)
+    local_tokens.start()
+    step(0)
+    local_tokens.wait()
+    spread(first, 0)
+    step(1)
+    step(2)
+    collect(first, 0)
+    norm_slots(first, pre_gain)
+    step(3)
+    step(4)
+    step(5)
+    ready(0)
+    ready(1)
+    gated(whole[0], whole[1], hidden_one)
+    spread(hidden_one, 1)
+    step(6)
+    collect(hidden_one, 1)
+    ready(2)
+    lower(hidden_one, whole[2], first, put(second))
+    spread(second, 2)
+    step(7)
+    collect(second, 2)
+    norm_slots(second, mix_gain)
+    ready(3)
+    tiles(SEQ_LEN, mix)
+    spread(channels, 3)
+    step(8)
+    collect(channels, 3)
+    norm_slots(channels, channel_gain)
+    ready(4)
+    tiles(ROW_TILE, project)
+    spread(third, 4)
+    step(9)
+    collect(third, 4)
+    norm_slots(third, post_gain)
+    for number in range(10, count + depth):
+        step(number)
+    ready(5)
+    ready(6)
+    gated(whole[5], whole[6], hidden_two)
+    spread(hidden_two, 5)
+    collect(hidden_two, 5)
+    ready(7)
+    lower(hidden_two, whole[7], third, finish)
+    links.drain()
+
+
+def fused(
+    fs_size,
+    tp_size,
+    tokens,
+    pre_gain,
+    pre_gate,
+    pre_up,
+    pre_down,
+    mix_gain,
+    branch_proj,
+    gate_proj,
+    conv_taps,
+    retain_blocks,
+    admit_blocks,
+    decay_param,
+    channel_gain,
+    out_proj,
+    post_gain,
+    post_gate,
+    post_up,
+    post_down,
+):
+    half_type = lambda array: array.astype(jnp.bfloat16)
+    shards = [
+        half_type(pre_gate),
+        half_type(pre_up),
+        half_type(pre_down),
+        jnp.concatenate((half_type(branch_proj), half_type(gate_proj)), axis=1),
+        half_type(out_proj),
+        half_type(post_gate),
+        half_type(post_up),
+        half_type(post_down),
+    ]
+    gates = jnp.concatenate((spread_blocks(retain_blocks), spread_blocks(admit_blocks)), axis=1)
+    sharpness = jax.nn.softplus(-decay_param)[None, :]
+    rows, width = tokens.shape
+    hidden = pre_gate.shape[1]
+    operands = [
+        tokens,
+        pre_gain[None],
+        mix_gain[None],
+        channel_gain[None],
+        post_gain[None],
+        conv_taps,
+        gates,
+        sharpness,
+        *shards,
+    ]
+    dma = pltpu.SemaphoreType.DMA
+    count = len(shards)
+    stacked = lambda columns: pltpu.VMEM((tp_size, rows, columns), jnp.bfloat16)
+    peers = max(tp_size // 2 - 1, 1)
+    return pl.pallas_call(
+        functools.partial(layer_kernel, fs_size, tp_size),
+        out_shape=jax.ShapeDtypeStruct(tokens.shape, tokens.dtype),
+        in_specs=[pl.BlockSpec(memory_space=pltpu.VMEM)] * len(operands),
+        out_specs=pl.BlockSpec(memory_space=pltpu.VMEM),
+        scratch_shapes=[
+            *(pltpu.VMEM((fs_size * s.shape[0], s.shape[1]), jnp.bfloat16) for s in shards),
+            stacked(width),
+            stacked(width),
+            stacked(width),
+            stacked(hidden),
+            stacked(hidden),
+            stacked(branch_proj.shape[1]),
+            pltpu.VMEM((rows, width * tp_size), jnp.bfloat16),
+            dma((count, fs_size)),
+            dma((count, fs_size)),
+            dma((count, 2)),
+            dma((count, fs_size // 2)),
+            dma((count,)),
+            dma((6, tp_size)),
+            dma((6, peers)),
+            dma((6,)),
+            dma((6, peers)),
+            dma,
+        ],
+        compiler_params=pltpu.CompilerParams(
+            collective_id=0, has_side_effects=True, vmem_limit_bytes=62 * 2**20
+        ),
+    )(*operands)
+
+
+def fits_fused(fs_size, tp_size, arrays):
+    shards = [a for i, a in enumerate(arrays) if i in (2, 3, 4, 6, 7, 13, 15, 16, 17)]
+    rows_fit = all(a.shape[0] % 16 == 0 for a in shards)
+    lanes_fit = all(arrays[i].shape[1] % 128 == 0 for i in (0, 6, 7))
+    tiles_fit = arrays[0].shape[0] % ROW_TILE == 0 and arrays[2].shape[1] % 16 == 0
+    return (
+        rows_fit
+        and lanes_fit
+        and tiles_fit
+        and fs_size % 2 == 0
+        and 4 <= fs_size <= 16
+        and tp_size % 2 == 0
+    )
+
+
 def local(
     tokens,
     pre_gain,
@@ -183,6 +568,13 @@
         P("fs", "tp"),
         P("fs", "tp"),
     )
+    fs_size, tp_size = mesh.shape["fs"], mesh.shape["tp"]
+
+    def layer(*arrays):
+        if fits_fused(fs_size, tp_size, arrays):
+            return fused(fs_size, tp_size, *arrays)
+        return local(*arrays)
+
     return jax.shard_map(
-        local, mesh=mesh, in_specs=placed, out_specs=P("fs", "tp"), check_vma=False
-    )
+        layer, mesh=mesh, in_specs=placed, out_specs=P("fs", "tp"), check_vma=False
+    )

time: 576 us -> 255 us (0.44)
  waiting for transfers between devices: 508 us -> 0 us
  Pallas kernels: 4.24 us -> 238 us
  matrix products: 29 us -> 0 us
  between operations: 13.8 us -> 0.07 us
  other arithmetic: 16.9 us -> 5.03 us
  local copies, waits for them, and re-layouts: 2.78 us -> 9.33 us
    all_gather x12 -> x0, waiting for transfers between devices: 507 us -> none  [the longest x6 376 us: contract(): lax.all_gather(stacked.astype(jnp.bfloat16), 'fs', axis=0, tiled=True)]
    pallas_call x1, Pallas kernels: 4.24 us -> 238 us  [fused(): pl.pallas_call(functools.partial(layer_kernel, fs_size, tp_size), out_sha...]
    dot_general x6 -> x0, matrix products: 29 us -> none  [contract(): jnp.dot(operand, lax.all_gather(stacked.astype(jnp.bfloat16), 'fs', axis=...]
    reduce_sum x4 -> x0, other arithmetic: 8.17 us -> none  [normalize(): jnp.mean(floats * floats, axis=-1, keepdims=True) + EPSILON]
  transfers between devices with their start and end apart: 12 -> 0, of which waited for: 12 -> 0; matrix products, arithmetic and copies ran while one was open for 5% -> 0% of each run, Pallas kernels for 0% -> 0%
where the time goes in v2:
time: 255 us; the launch traced here: 253 us
  Pallas kernels  238 us (93%)
  local copies, waits for them, and re-layouts  9.33 us (4%)
  other arithmetic  5.03 us (2%)
    pallas_call x1, Pallas kernels, fused(): pl.pallas_call(functools.partial(layer_kernel, fs_size, tp_size), out_sha...  238 us
    unnamed x21, local copies, waits for them, and re-layouts  5.22 us

profile of v2, /device:TPU:0, one launch (start us, length us, event | category | flops | bytes accessed | tf_op | source)
XLA Modules:
  0.0 252.9 jit_solution(7829075735802976751)
XLA Ops:
  0.0 1.2 multiply_convert_fusion.1
  1.2 0.2 convert_element_type.51
  1.5 0.0 copy-start.6
  1.5 0.2 convert_element_type.53
  1.7 0.7 copy-done.6
  2.4 0.0 copy-start.7
  2.4 0.9 copy-done.7
  3.4 0.9 pad_maximum_fusion
  4.2 0.4 copy-done
  4.7 0.0 copy-start.1
  4.7 0.9 copy.23.refs_8_
  5.6 0.1 copy-done.1
  5.8 0.0 copy-start.2
  5.8 0.9 copy.24.refs_9_
  6.7 0.2 copy-done.2
  6.9 0.9 copy.25.refs_13_
  7.8 0.1 copy-done.3
  8.0 0.0 copy-start.4
  8.0 0.9 copy.26.refs_14_
  8.9 0.1 copy-done.4
  9.1 0.0 copy-start.5
  9.1 0.8 convert_element_type.56.refs_10_
  9.9 0.5 copy-done.5
  10.3 0.0 copy-start.8
  10.3 0.8 convert_element_type.62.refs_15_
  11.1 0.2 copy-done.8
  11.3 0.0 copy-start.9
  11.3 0.7 convert_element_type.59.refs_12_
  12.0 0.0 copy-done.9
  12.0 0.6 compare_select_fusion
  12.5 238.5 %shard_map.172 = bf16[512,512]{1,0:T(8,128)(2,1)} custom-call(bf16[512,512]{1,0:T(8,128)(2,1)} %refs_0_.1, f32[1,2048]{1,0:T(1,128)} %bitcast.5, f32[1,2048]{1,0:T(1,128)} %bitcast.6, f32[1,1024]{1,0:T(1,128)} %bitcast.8, f32[1,2048]{1,0:T(1,128)} %bitcast.7, f32[4,256]{1,0:T(4,128)} %refs_5_.1, bf16[256,512]{1,0:T(8,128)(2,1)} %get-tuple-element.7.refs_6_, ...), custom_call_target="tpu_custom_call" | custom-call | tf_op jit(solution)/shard_map/pallas_call | solution.py:468
  251.0 1.9 copy.28
  (9 shorter events, 0.2 us)
Async XLA Ops:
  1.5 1.0 copy-start.6
  2.4 0.9 copy-start.7
  3.4 1.3 copy-start
  4.7 1.1 copy-start.1
  5.8 1.1 copy-start.2
  6.9 1.1 copy-start.3
  8.0 1.1 copy-start.4
  9.1 1.2 copy-start.5
  10.3 1.0 copy-start.8
  11.3 0.7 copy-start.9

commit v3 on v2

--- a/solution.py
+++ b/solution.py
@@ -324,9 +324,22 @@
         return jnp.dot(left, right, preferred_element_type=jnp.float32)
 
     def gated(gate, up, hidden):
+        features = gate.shape[1]
+        width = hidden.shape[2]
+
+        def turned(rows, matrix):
+            return sum(
+                lax.dot_general(
+                    normed[rows, s * features : (s + 1) * features],
+                    matrix[s * width : (s + 1) * width, :],
+                    (((1,), (1,)), ((), ())),
+                    preferred_element_type=jnp.float32,
+                )
+                for s in range(fs_size)
+            )
+
         def body(rows):
-            values = normed[rows, :]
-            product = jax.nn.silu(dot(values, gate[...])) * dot(values, up[...])
+            product = jax.nn.silu(turned(rows, gate)) * turned(rows, up)
             hidden[t, rows, :] = product.astype(jnp.bfloat16)
 
         tiles(ROW_TILE, body)
@@ -401,12 +414,14 @@
     step(9)
     collect(third, 4)
     norm_slots(third, post_gain)
-    for number in range(10, count + depth):
+    for number in range(10, count + depth - 2):
         step(number)
     ready(5)
     ready(6)
     gated(whole[5], whole[6], hidden_two)
     spread(hidden_two, 5)
+    for number in range(max(10, count + depth - 2), count + depth):
+        step(number)
     collect(hidden_two, 5)
     ready(7)
     lower(hidden_two, whole[7], third, finish)
@@ -437,13 +452,13 @@
 ):
     half_type = lambda array: array.astype(jnp.bfloat16)
     shards = [
-        half_type(pre_gate),
-        half_type(pre_up),
+        half_type(pre_gate.T),
+        half_type(pre_up.T),
         half_type(pre_down),
         jnp.concatenate((half_type(branch_proj), half_type(gate_proj)), axis=1),
         half_type(out_proj),
-        half_type(post_gate),
-        half_type(post_up),
+        half_type(post_gate.T),
+        half_type(post_up.T),
         half_type(post_down),
     ]
     gates = jnp.concatenate((spread_blocks(retain_blocks), spread_blocks(admit_blocks)), axis=1)
@@ -501,10 +516,12 @@
     rows_fit = all(a.shape[0] % 16 == 0 for a in shards)
     lanes_fit = all(arrays[i].shape[1] % 128 == 0 for i in (0, 6, 7))
     tiles_fit = arrays[0].shape[0] % ROW_TILE == 0 and arrays[2].shape[1] % 16 == 0
+    turned_fit = all(arrays[i].shape[0] % 128 == 0 for i in (2, 3, 15, 16))
     return (
         rows_fit
         and lanes_fit
         and tiles_fit
+        and turned_fit
         and fs_size % 2 == 0
         and 4 <= fs_size <= 16
         and tp_size % 2 == 0

time: 255 us -> 243 us (0.953)
  Pallas kernels: 238 us -> 229 us
  local copies, waits for them, and re-layouts: 9.33 us -> 3.73 us
  other arithmetic: 5.03 us -> 8.5 us
    pallas_call x1, Pallas kernels: 238 us -> 229 us  [fused(): pl.pallas_call(functools.partial(layer_kernel, fs_size, tp_size), out_sha...]
    convert_element_type x9 -> x7, other arithmetic: 2.4 us -> 6.1 us  [fused(): half_type = lambda array: array.astype(jnp.bfloat16)]
    convert_element_type x4 -> x0, local copies, waits for them, and re-layouts: 3.68 us -> none  [fused(): half_type = lambda array: array.astype(jnp.bfloat16)]
    unnamed x21 -> x19, local copies, waits for them, and re-layouts: 5.22 us -> 3.3 us
where the time goes in v3:
time: 243 us; the launch traced here: 241 us
  Pallas kernels  229 us (94%)
  other arithmetic  8.5 us (3%)
  local copies, waits for them, and re-layouts  3.73 us (2%)
    pallas_call x1, Pallas kernels, fused(): pl.pallas_call(functools.partial(layer_kernel, fs_size, tp_size), out_sha...  229 us
    convert_element_type x7, other arithmetic, fused(): half_type = lambda array: array.astype(jnp.bfloat16)  6.1 us

profile of v3, /device:TPU:0, one launch (start us, length us, event | category | flops | bytes accessed | tf_op | source)
XLA Modules:
  0.0 241.0 jit_solution(15372791506773099561)
XLA Ops:
  0.0 0.0 copy-start.6
  0.0 0.0 copy-start
  0.0 1.3 compare_select_fusion
  1.3 1.0 convert_element_type.67
  2.3 0.0 copy-done.6
  2.3 0.0 copy-start.1
  2.3 1.7 convert_element_type.69.refs_12_
  4.0 0.0 copy-done
  4.0 0.8 convert_element_type.66.refs_10_
  4.8 0.0 copy-done.1
  4.8 0.0 copy-start.7
  4.8 0.0 copy-start.8
  4.8 0.8 convert_element_type.74.refs_15_
  5.6 0.1 copy-done.7
  5.7 0.2 copy-done.8
  5.9 0.3 multiply_convert_fusion.1
  6.2 0.2 convert_element_type.59
  6.4 0.0 copy-start.2
  6.4 0.0 copy-start.3
  6.4 0.2 convert_element_type.61
  6.6 0.8 pad_maximum_fusion
  7.5 0.0 copy-done.2
  7.5 0.4 copy-done.3
  7.9 0.0 copy-start.4
  7.9 0.0 copy-start.5
  7.9 0.9 convert_bitcast_fusion.2
  8.8 0.4 copy-done.4
  9.3 0.2 copy-done.5
  9.5 0.9 convert_bitcast_fusion
  10.4 228.7 %shard_map.172 = bf16[512,512]{1,0:T(8,128)(2,1)} custom-call(bf16[512,512]{1,0:T(8,128)(2,1)} %refs_0_.1, f32[1,2048]{1,0:T(1,128)} %bitcast.13, f32[1,2048]{1,0:T(1,128)} %bitcast.14, f32[1,1024]{1,0:T(1,128)} %bitcast.17, f32[1,2048]{1,0:T(1,128)} %bitcast.15, f32[4,256]{1,0:T(4,128)} %refs_5_.1, bf16[256,512]{1,0:T(8,128)(2,1)} %get-tuple-element.11.refs_6_, ...), custom_call_target="tpu_custom_call" | custom-call | tf_op jit(solution)/shard_map/pallas_call | solution.py:483
  239.1 1.9 copy.20
  (2 shorter events, 0.0 us)
Async XLA Ops:
  0.0 2.3 copy-start.6
  0.0 4.0 %copy-start = (f32[352,512]{1,0:T(8,128)S(1)}, f32[352,512]{1,0:T(8,128)}, u32[]{:S(2)}) copy-start(f32[352,512]{1,0:T(8,128)} %param.22) | copy-start | bytes 2162692
  2.3 2.5 %copy-start.1 = (f32[352,512]{1,0:T(8,128)S(1)}, f32[352,512]{1,0:T(8,128)}, u32[]{:S(2)}) copy-start(f32[352,512]{1,0:T(8,128)} %param.35) | copy-start | bytes 2162692
  4.8 0.9 copy-start.7
  4.8 1.1 copy-start.8
  6.4 1.1 copy-start.2
  6.4 1.5 copy-start.3
  7.9 1.4 copy-start.4
  7.9 1.6 copy-start.5
